TPU v7x, 32 devices: a whole 2x2x4 slice. The times are simulated.
32 devices in a mesh: sp: 8 (over z, x), tp: 4 (over y, core).
Axes of the slice: x: 2, y: 2, z: 4, core: 2. Of those that a mesh axis runs over, the one named last changes fastest.
Arguments:
- moe_in: bfloat16 [1536, 2048], P('sp', 'tp'), may hold values from -6 to 6
- cotangent: bfloat16 [1536, 2048], P('sp', 'tp'), may hold values from -6 to 6
- routes: int32 [1536, 2], P('sp'), may hold values from 0 to 7, all different within a row; in each aligned block of 192 rows (0 to 191, 192 to 383, ...) at most 60 rows name the same one
- route_weight: float32 [1536, 2], P('sp'), may hold values from 0.2 to 1
- w_gate: bfloat16 [8, 3584, 2048], P('sp', 'tp'), may hold values from -0.125 to 0.125
- w_up: bfloat16 [8, 3584, 2048], P('sp', 'tp'), may hold values from -0.125 to 0.125
- w_down: bfloat16 [8, 3584, 2048], P('sp', 'tp'), may hold values from -0.09375 to 0.09375
- conv_pre: bfloat16 [1536, 2048], P('sp', 'tp'), may hold values from -6 to 6
- norm_mean: float32 [1536], P('sp'), may hold values from -3 to 3
- norm_rstd: float32 [1536], P('sp'), may hold values from 0.5 to 2
- ln_gain: float32 [2048], P('tp'), may hold values from 0.1 to 1.9
- ln_shift: float32 [2048], P('tp'), may hold values from -3 to 3
- taps: float32 [31, 2048], P(None, 'tp'), may hold values from -1 to 1
- w_proj: bfloat16 [2048, 2048], P('sp', 'tp'), may hold values from -0.125 to 0.125
Outputs:
- grad_up: bfloat16 [8, 3584, 2048], P('sp', 'tp')
- grad_down: bfloat16 [8, 3584, 2048], P('sp', 'tp')
- grad_stream: bfloat16 [1536, 2048], P('sp', 'tp')
- grad_proj: float32 [2048, 2048], P('sp', 'tp')
- grad_conv: bfloat16 [1536, 2048], P('sp', 'tp')
Inputs may be any that keep to these rules, and one draw needn't show every extreme that they name: `routes`: each token names 2 different experts. Among the tokens of one index of sp no expert is named more than 60 times, a bound that some block reaches.
All inputs are finite; a program needn't handle non-finite values.
Results may differ from a plain program's by a relative error of at most 0.02.
Values may be sent and summed in bfloat16 or wider, within the bound.
A program may use at most 64 MiB of HBM per device.

v0:
```python
import jax
import jax.numpy as jnp
from jax import lax
from jax.sharding import PartitionSpec as P


def passed_along(value, axis, steps):
    count = lax.axis_size(axis)
    first, last = (max(0, -steps), min(count, count - steps))
    return lax.ppermute(value, axis, [(source, source + steps) for source in range(first, last)])


def silu_slope(pre_value, sigmoid_value):
    return sigmoid_value * (1.0 + pre_value * (1.0 - sigmoid_value))


def expert_backward(expert_rows, routed_rows, gate_weight, up_weight, down_weight):
    gate_pre = lax.dot_general(
        expert_rows, gate_weight, (((1,), (1,)), ((), ())), preferred_element_type=jnp.float32
    )
    up_pre = lax.dot_general(
        expert_rows, up_weight, (((1,), (1,)), ((), ())), preferred_element_type=jnp.float32
    )
    gate_sigmoid = jax.nn.sigmoid(gate_pre)
    gate_active = gate_pre * gate_sigmoid
    hidden = (gate_active * up_pre).astype(jnp.bfloat16)
    hidden_grad = lax.dot_general(
        routed_rows, down_weight, (((1,), (1,)), ((), ())), preferred_element_type=jnp.float32
    )
    grad_down = lax.dot_general(
        hidden, routed_rows, (((0,), (0,)), ((), ())), preferred_element_type=jnp.float32
    ).astype(jnp.bfloat16)
    gate_grad = (hidden_grad * up_pre * silu_slope(gate_pre, gate_sigmoid)).astype(jnp.bfloat16)
    up_grad = (hidden_grad * gate_active).astype(jnp.bfloat16)
    grad_up = lax.dot_general(
        up_grad, expert_rows, (((0,), (0,)), ((), ())), preferred_element_type=jnp.float32
    ).astype(jnp.bfloat16)
    partial_rows = jnp.dot(gate_grad, gate_weight, preferred_element_type=jnp.float32)
    partial_rows = partial_rows + jnp.dot(up_grad, up_weight, preferred_element_type=jnp.float32)
    return (grad_up[None], grad_down[None], partial_rows)


def on_device(
    moe_in,
    cotangent,
    routes,
    route_weight,
    w_gate,
    w_up,
    w_down,
    conv_pre,
    norm_mean,
    norm_rstd,
    ln_gain,
    ln_shift,
    taps,
    w_proj,
):
    devices = lax.axis_size("sp")
    local_tokens = routes.shape[0]
    top_count = routes.shape[1]
    channels = moe_in.shape[1]
    capacity = 5 * local_tokens // (2 * devices)
    route_ids = routes.reshape(-1)
    onehot = (route_ids[:, None] == jnp.arange(devices, dtype=jnp.int32)[None, :]).astype(jnp.int32)
    earlier = jnp.cumsum(onehot, axis=0) - onehot
    targets = route_ids * capacity + jnp.sum(earlier * onehot, axis=1)
    positions = jnp.arange(devices * capacity, dtype=jnp.int32)
    matches = targets[None, :] == positions[:, None]
    filled = jnp.any(matches, axis=1)[:, None]
    pair_index = jnp.arange(targets.shape[0], dtype=jnp.int32)
    route_of_slot = jnp.sum(jnp.where(matches, pair_index[None, :], 0), axis=1)
    zero_value = jnp.zeros((), jnp.bfloat16)
    routed = (route_weight[:, :, None] * cotangent.astype(jnp.float32)[:, None, :]).astype(
        jnp.bfloat16
    )
    routed = routed.reshape(local_tokens * top_count, cotangent.shape[1])
    send_rows = jnp.where(filled, jnp.take(moe_in, route_of_slot // top_count, axis=0), zero_value)
    send_routed = jnp.where(filled, jnp.take(routed, route_of_slot, axis=0), zero_value)
    send_rows, send_routed = (send_rows, send_routed)
    part_rows, part_routed = (
        lax.all_to_all(send_rows, "sp", split_axis=0, concat_axis=0, tiled=True),
        lax.all_to_all(send_routed, "sp", split_axis=0, concat_axis=0, tiled=True),
    )
    expert_rows, routed_rows = (
        lax.all_gather(part_rows, "tp", axis=1, tiled=True),
        lax.all_gather(part_routed, "tp", axis=1, tiled=True),
    )
    grad_up, grad_down, partial_rows = expert_backward(
        expert_rows, routed_rows, w_gate[0], w_up[0], w_down[0]
    )
    shared = lax.psum_scatter(
        partial_rows.astype(jnp.bfloat16).astype(jnp.float32).astype(jnp.bfloat16),
        "tp",
        scatter_dimension=1,
        tiled=True,
    )
    returned = lax.all_to_all(shared, "sp", split_axis=0, concat_axis=0, tiled=True)
    picked = jnp.take(returned, targets, axis=0).astype(jnp.float32)
    grad_stream = (
        cotangent.astype(jnp.float32)
        + jnp.sum(picked.reshape(local_tokens, top_count, returned.shape[1]), axis=1)
    ).astype(jnp.bfloat16)
    mix_grad = lax.all_gather(grad_stream, "tp", axis=1, tiled=True)
    normed = (conv_pre.astype(jnp.float32) - norm_mean[:, None]) * norm_rstd[:, None]
    pre_act = normed * ln_gain[None, :] + ln_shift[None, :]
    act_sigmoid = jax.nn.sigmoid(pre_act)
    activated = (pre_act * act_sigmoid).astype(jnp.bfloat16)
    columns = mix_grad
    act_grad = jnp.dot(
        columns,
        lax.all_gather(w_proj, "sp", axis=0, tiled=True),
        preferred_element_type=jnp.float32,
    )
    columns = mix_grad
    grad_proj = lax.psum_scatter(
        lax.dot_general(
            columns, activated, (((0,), (0,)), ((), ())), preferred_element_type=jnp.float32
        ).astype(jnp.bfloat16),
        "sp",
        scatter_dimension=0,
        tiled=True,
    ).astype(jnp.float32)
    normed_grad = act_grad * silu_slope(pre_act, act_sigmoid) * ln_gain[None, :]
    first_sum, second_sum = lax.psum(
        (jnp.sum(normed_grad, axis=1), jnp.sum(normed_grad * normed, axis=1)), "tp"
    )
    width = channels * lax.axis_size("tp")
    conv_grad = norm_rstd[:, None] * (
        normed_grad - first_sum[:, None] / width - normed * (second_sum[:, None] / width)
    )
    lag_count = taps.shape[0]
    rim_rows = passed_along(conv_grad[: lag_count - 1], "sp", -1)
    extended = jnp.concatenate([conv_grad, rim_rows], axis=0)
    grad_conv = jnp.zeros((local_tokens, channels), jnp.float32)
    for lag in range(lag_count):
        grad_conv = grad_conv + taps[lag][None, :] * extended[lag : lag + local_tokens]
    return (grad_up, grad_down, grad_stream, grad_proj, grad_conv.astype(jnp.bfloat16))


def solution(mesh):
    placed = (
        P("sp", "tp"),
        P("sp", "tp"),
        P("sp", None),
        P("sp", None),
        P("sp", "tp", None),
        P("sp", "tp", None),
        P("sp", "tp", None),
        P("sp", "tp"),
        P("sp"),
        P("sp"),
        P("tp"),
        P("tp"),
        P(None, "tp"),
        P("sp", "tp"),
    )
    return jax.shard_map(
        on_device,
        mesh=mesh,
        in_specs=placed,
        out_specs=(
            P("sp", "tp", None),
            P("sp", "tp", None),
            P("sp", "tp"),
            P("sp", "tp"),
            P("sp", "tp"),
        ),
        check_vma=False,
    )
```

profile of v0, /device:TPU:0, one launch (start us, length us, event | category | flops | bytes accessed | tf_op | source)
XLA Modules:
  0.0 252.3 jit_solution(15839050493758933226)
XLA Ops:
  8.1 0.8 copy.28
  8.9 0.1 eq.39
  9.0 0.1 reshape.200
  9.2 0.9 reduce-window.6
  10.0 0.2 slice_reduce_fusion
  10.3 0.1 fusion.113
  10.4 0.2 select_reduce_fusion
  10.6 0.2 fusion.15
  10.7 0.1 reduce_sum.55
  10.8 1.1 mul.435
  12.0 0.5 mul.436
  12.5 0.1 copy.30
  12.7 0.1 mul.433
  12.8 0.1 multiply_convert_fusion.5
  12.9 2.1 gather_fusion
  15.1 0.1 gather.19
  15.2 2.1 gather_fusion.1
  17.3 0.1 gather.21
  17.4 0.1 broadcast_in_dim.79
  17.5 0.3 select_select_fusion
  17.8 21.6 %all_to_all.30 = bf16[8,60,512]{2,1,0:T(8,128)(2,1)S(1)} all-to-all(bf16[8,60,512]{2,1,0:T(8,128)(2,1)S(1)} %get-tuple-element.44), channel_id=1, replica_groups=mesh['sp'=8,'tp'=4] {'sp'}, dimensions={0} | all-to-all | bytes 983040 | tf_op jit(solution)/shard_map/all_to_all | solution.py:82
  39.4 0.9 all_to_all.23
  40.3 0.0 all-gather.4.cloned.1.call-start
  40.4 17.5 %all_to_all.31 = bf16[8,60,512]{2,1,0:T(8,128)(2,1)S(1)} all-to-all(bf16[8,60,512]{2,1,0:T(8,128)(2,1)S(1)} %get-tuple-element.45), channel_id=1, replica_groups=mesh['sp'=8,'tp'=4] {'sp'}, dimensions={0} | all-to-all | bytes 983040 | tf_op jit(solution)/shard_map/all_to_all | solution.py:83
  57.9 0.9 all_to_all.21
  58.8 0.2 reduce-scatter.3.cloned.1.call-start
  59.0 2.3 all-gather.6.cloned.1.call-done
  61.4 4.9 %fusion.6 = f32[480,896]{1,0:T(8,128)S(1)} fusion(bf16[480,2048]{1,0:T(8,128)(2,1)} %all-gather.6.cloned.1.call-done, bf16[1,896,2048]{2,1,0:T(8,128)(2,1)} %param.18), kind=kOutput, calls=%fused_computation.39 | convolution fusion | flops 1761607680 | bytes 7356416 | tf_op jit(solution)/shard_map/dot_general | solution.py:18
  66.2 19.1 %all-gather.4.cloned.1.call-done = bf16[480,2048]{1,0:T(8,128)(2,1)} async-done(((bf16[480,512]{1,0:T(8,128)(2,1)}), bf16[480,2048]{1,0:T(8,128)(2,1)}) %all-gather.4.cloned.1.call-update) | async-done | bytes 1966096 | tf_op jit(solution)/shard_map/all_gather | solution.py:87
  85.4 5.1 %multiply_convert_fusion.2 = (bf16[480,896]{1,0:T(8,128)(2,1)S(1)}, f32[480,896]{1,0:T(8,128)S(1)}) fusion(f32[480,896]{1,0:T(8,128)S(1)} %fusion.6, bf16[480,2048]{1,0:T(8,128)(2,1)} %all-gather.4.cloned.1.call-done, bf16[1,896,2048]{2,1,0:T(8,128)(2,1)} %param.20), kind=kOutput, calls=%fused_computation.48 | convolution fusion | flops 1764188160 | bytes 9936896 | tf_op jit(solution)/shard_map/dot_general | solution.py:27
  90.5 0.9 copy-done.17
  91.4 2.2 fusion
  93.6 2.3 fusion.2
  95.9 1.2 copy-done.16
  97.1 3.7 %add_convert_fusion = bf16[480,2048]{1,0:T(8,128)(2,1)} fusion(f32[480,2048]{1,0:T(8,128)S(1)} %fusion, bf16[1,896,2048]{2,1,0:T(8,128)(2,1)S(1)} %copy-done.10, f32[480,896]{1,0:T(8,128)S(1)} %fusion.6, f32[480,896]{1,0:T(8,128)S(1)} %get-tuple-element.47, f32[480,896]{1,0:T(8,128)S(1)} %fusion.2), kind=kOutput, calls=%fused_computation.32 | convolution fusion | flops 1767874560 | bytes 14729216 | tf_op jit(solution)/shard_map/dot_general | solution.py:38
  100.9 0.0 all-gather.8.cloned.1.call-start
  100.9 0.5 all-gather.8.cloned.1.call-update
  101.4 30.0 %reduce-scatter.3.cloned.1.call-done = bf16[480,512]{1,0:T(8,128)(2,1)} async-done(((bf16[480,2048]{1,0:T(8,128)(2,1)}), bf16[480,512]{1,0:T(8,128)(2,1)}) %reduce-scatter.3.cloned.1.call-update) | async-done | bytes 491536 | tf_op jit(solution)/shard_map/reduce_scatter | solution.py:92
  131.4 1.9 all_to_all.24
  133.3 5.5 %all-to-all-start.2 = ((bf16[8,60,512]{2,1,0:T(8,128)(2,1)}), bf16[8,60,512]{2,1,0:T(8,128)(2,1)S(1)}, u32[]{:S(2)}, u32[]{:S(2)}) async-start(bf16[8,60,512]{2,1,0:T(8,128)(2,1)} %all_to_all.24), calls=%async_computation.3 | async-start | bytes 1048576 | tf_op jit(solution)/shard_map/all_to_all | solution.py:98
  138.8 0.0 reduce-scatter.5.cloned.1.call-start
  138.9 0.1 reduce_sum.57
  139.0 0.1 copy.33
  139.2 0.1 mul.447
  139.3 0.1 copy.31
  139.4 0.2 copy.32
  139.6 21.8 %all-to-all-done.2 = bf16[8,60,512]{2,1,0:T(8,128)(2,1)S(1)} async-done(((bf16[8,60,512]{2,1,0:T(8,128)(2,1)}), bf16[8,60,512]{2,1,0:T(8,128)(2,1)S(1)}, u32[]{:S(2)}, u32[]{:S(2)}) %all-to-all-start.2) | async-done | bytes 491552 | tf_op jit(solution)/shard_map/all_to_all | solution.py:98
  161.4 0.1 all_to_all.26
  161.5 2.1 gather_fusion.2
  163.6 0.2 gather.23
  163.8 1.1 convert_reduce_fusion
  165.0 8.4 %all_gather.14 = bf16[192,2048]{1,0:T(8,128)(2,1)S(1)} all-gather(bf16[192,512]{1,0:T(8,128)(2,1)S(1)} %add_convert_fusion.1), channel_id=1, replica_groups=mesh['sp'=8,'tp'=4] {'tp'}, dimensions={1}, use_global_device_ids=true | all-gather | bytes 983040 | tf_op jit(solution)/shard_map/all_gather | solution.py:104
  173.4 2.3 convolution_convert_fusion
  175.7 0.8 copy-done.4
  176.6 0.7 copy-done.12
  177.3 6.0 %convert_bitcast_fusion = bf16[1,896,2048]{2,1,0:T(8,128)(2,1)} fusion(bf16[480,2048]{1,0:T(8,128)(2,1)S(1)} %copy-done.12, f32[480,896]{1,0:T(8,128)} %copy-done.16, f32[480,896]{1,0:T(8,128)} %copy-done.15), kind=kOutput, calls=%fused_computation.43 | convolution fusion | flops 1766023168 | bytes 9076736 | tf_op jit(solution)/shard_map/dot_general | solution.py:30
  183.3 2.5 fusion.121
  185.8 7.0 %all-reduce = (f32[192]{0:T(256)S(1)}, f32[192]{0:T(256)S(1)}) all-reduce(f32[192]{0:T(256)S(1)} %get-tuple-element.6, f32[192]{0:T(256)S(1)} %get-tuple-element.5), channel_id=1, replica_groups=mesh['sp'=8,'tp'=4] {'tp'}, use_global_device_ids=true, to_apply=%region_11.12 | all-reduce | flops 384 | bytes 3072 | tf_op jit(solution)/shard_map/psum | solution.py:125
  192.7 0.2 subtract_multiply_fusion
  192.9 1.3 collective-permute-start
  194.2 5.5 %convert_bitcast_fusion.1 = bf16[1,896,2048]{2,1,0:T(8,128)(2,1)} fusion(bf16[480,896]{1,0:T(8,128)(2,1)S(1)} %copy-done.18, bf16[480,2048]{1,0:T(8,128)(2,1)} %all-gather.6.cloned.1.call-done), kind=kOutput, calls=%fused_computation.44 | convolution fusion | flops 1763442688 | bytes 6496256 | tf_op jit(solution)/shard_map/dot_general | solution.py:35
  199.8 2.5 fusion.20
  202.3 41.1 %reduce-scatter.5.cloned.1.call-done = bf16[256,512]{1,0:T(8,128)(2,1)} async-done(((bf16[2048,512]{1,0:T(8,128)(2,1)}), bf16[256,512]{1,0:T(8,128)(2,1)}) %reduce-scatter.5.cloned.1.call-update) | async-done | bytes 262160 | tf_op jit(solution)/shard_map/reduce_scatter | solution.py:116
  243.4 1.8 convert_element_type.72
  (57 shorter events, 0.5 us)
Async XLA Ops:
  8.0 7.2 %copy-start = (bf16[192,512]{1,0:T(8,128)(2,1)S(1)}, bf16[192,512]{1,0:T(8,128)(2,1)}, u32[]{:S(2)}) copy-start(bf16[192,512]{1,0:T(8,128)(2,1)} %param.14) | copy-start | bytes 589828
  8.0 4.5 %copy-start.6 = (f32[192,2]{0,1:T(2,128)S(1)}, f32[192,2]{0,1:T(2,128)}, u32[]{:S(2)}) copy-start(f32[192,2]{0,1:T(2,128)} %param.17) | copy-start | bytes 4612
  8.0 53.3 %all-gather.6.cloned.1.call-start = ((), (), s32[]{:S(2)}) async-start(), calls=%async_computation.6 | async-start | bytes 2457600 | tf_op jit(solution)/shard_map/all_gather | solution.py:86
  40.3 45.0 %all-gather.4.cloned.1.call-start = ((), (), s32[]{:S(2)}) async-start(), calls=%async_computation.5 | async-start | bytes 2457600 | tf_op jit(solution)/shard_map/all_gather | solution.py:87
  58.8 72.6 %reduce-scatter.3.cloned.1.call-start = ((), (), s32[]{:S(2)}) async-start(), calls=%async_computation.7 | async-start | bytes 2457600 | tf_op jit(solution)/shard_map/reduce_scatter | solution.py:92
  66.2 29.7 %copy-start.15 = (f32[480,896]{1,0:T(8,128)}, f32[480,896]{1,0:T(8,128)S(1)}, u32[]{:S(2)}) copy-start(f32[480,896]{1,0:T(8,128)S(1)} %fusion.6) | copy-start | bytes 5160964
  85.3 6.0 %copy-start.9 = (bf16[1,896,2048]{2,1,0:T(8,128)(2,1)S(1)}, bf16[1,896,2048]{2,1,0:T(8,128)(2,1)}, u32[]{:S(2)}) copy-start(bf16[1,896,2048]{2,1,0:T(8,128)(2,1)} %param.19) | copy-start | bytes 11010052
  90.5 0.9 copy-start.17
  91.4 2.2 copy-start.11
  93.6 3.5 %copy-start.10 = (bf16[1,896,2048]{2,1,0:T(8,128)(2,1)S(1)}, bf16[1,896,2048]{2,1,0:T(8,128)(2,1)}, u32[]{:S(2)}) copy-start(bf16[1,896,2048]{2,1,0:T(8,128)(2,1)} %param.18) | copy-start | bytes 11010052
  95.9 1.2 copy-start.16
  100.8 38.2 %copy-start.5 = (s32[192,2]{0,1:T(2,128)S(1)}, s32[192,2]{0,1:T(2,128)}, u32[]{:S(2)}) copy-start(s32[192,2]{0,1:T(2,128)} %param.16) | copy-start | bytes 4612
  100.9 82.4 %all-gather.8.cloned.1.call-start = ((), (), s32[]{:S(2)}) async-start(), calls=%async_computation.9 | async-start | bytes 2359296 | tf_op jit(solution)/shard_map/all_gather | solution.py:112
  133.3 28.1 %all-to-all-start.2 = ((bf16[8,60,512]{2,1,0:T(8,128)(2,1)}), bf16[8,60,512]{2,1,0:T(8,128)(2,1)S(1)}, u32[]{:S(2)}, u32[]{:S(2)}) async-start(bf16[8,60,512]{2,1,0:T(8,128)(2,1)} %all_to_all.24), calls=%async_computation.3 | async-start | bytes 1048576 | tf_op jit(solution)/shard_map/all_to_all | solution.py:98
  138.8 104.6 %reduce-scatter.5.cloned.1.call-start = ((), (), s32[]{:S(2)}) async-start(), calls=%async_computation.8 | async-start | bytes 2359296 | tf_op jit(solution)/shard_map/reduce_scatter | solution.py:116
  161.5 3.4 %copy-start.1 = (bf16[192,512]{1,0:T(8,128)(2,1)S(1)}, bf16[192,512]{1,0:T(8,128)(2,1)}, u32[]{:S(2)}) copy-start(bf16[192,512]{1,0:T(8,128)(2,1)} %param.15) | copy-start | bytes 589828
  163.6 9.8 %copy-start.3 = (bf16[192,512]{1,0:T(8,128)(2,1)S(1)}, bf16[192,512]{1,0:T(8,128)(2,1)}, u32[]{:S(2)}) copy-start(bf16[192,512]{1,0:T(8,128)(2,1)} %param.21) | copy-start | bytes 589828
  163.6 9.8 %copy-start.7 = (f32[192]{0:T(256)S(1)}, f32[192]{0:T(256)}, u32[]{:S(2)}) copy-start(f32[192]{0:T(256)} %param.23) | copy-start | bytes 2308
  163.6 9.8 %copy-start.8 = (f32[192]{0:T(256)S(1)}, f32[192]{0:T(256)}, u32[]{:S(2)}) copy-start(f32[192]{0:T(256)} %param.22) | copy-start | bytes 2308
  163.6 9.8 %copy-start.13 = (f32[512]{0:T(512)S(1)}, f32[512]{0:T(512)}, u32[]{:S(2)}) copy-start(f32[512]{0:T(512)} %param.25) | copy-start | bytes 6148
  163.6 9.8 %copy-start.14 = (f32[512]{0:T(512)S(1)}, f32[512]{0:T(512)}, u32[]{:S(2)}) copy-start(f32[512]{0:T(512)} %param.24) | copy-start | bytes 6148
  165.0 10.7 %copy-start.2 = (bf16[192,512]{1,0:T(8,128)(2,1)}, bf16[192,512]{1,0:T(8,128)(2,1)S(1)}, u32[]{:S(2)}) copy-start(bf16[192,512]{1,0:T(8,128)(2,1)S(1)} %add_convert_fusion.1) | copy-start | bytes 589828
  175.7 0.8 copy-start.4
  175.7 1.6 copy-start.12
  183.3 10.9 %copy-start.18 = (bf16[480,896]{1,0:T(8,128)(2,1)S(1)}, bf16[480,896]{1,0:T(8,128)(2,1)}, u32[]{:S(2)}) copy-start(bf16[480,896]{1,0:T(8,128)(2,1)} %copy-done.17) | copy-start | bytes 2580484
  192.9 6.9 %collective-permute-start = (f32[30,512]{1,0:T(8,128)S(1)}, f32[30,512]{1,0:T(8,128)S(1)}, u32[]{:S(2)}, u32[]{:S(2)}) collective-permute-start(f32[30,512]{1,0:T(8,128)S(1)} %slice.263), channel_id=1, source_target_pairs={{4,0},{8,4},{12,8},{16,12},{20,16},{24,20},{28,24},{5,1},{9,5},{13... | collective-permute-start | bytes 184328 | tf_op jit(solution)/shard_map/ppermute | solution.py:10
Sparse Core Ops, SparseCore 0:
  40.4 20.8 all-gather.5
  63.5 21.8 all-gather.3
  101.0 30.3 reduce-scatter.2
Sparse Core Ops, SparseCore 1:
  103.5 58.3 all-gather.7
  175.8 67.5 reduce-scatter.4
where the time goes:
time: 253 us; the launch traced here: 252 us
  waiting for transfers between devices  115 us (45%)
  blocking collectives  54.5 us (22%)
  matrix products  34.5 us (14%)
  local copies, waits for them, and re-layouts  18.2 us (7%)
  between operations  15.6 us (6%)
  other arithmetic  7.48 us (3%)
  starting transfers between devices  7.19 us (3%)
    reduce_scatter x1, waiting for transfers between devices, on_device(): lax.psum_scatter(lax.dot_general(columns, activated, (((0,), (0,)), ((),...  41.1 us
    reduce_scatter x1, waiting for transfers between devices, on_device(): lax.psum_scatter(partial_rows.astype(jnp.bfloat16).astype(jnp.float32).as...  30 us
    all_to_all x1, waiting for transfers between devices, on_device(): lax.all_to_all(shared, 'sp', split_axis=0, concat_axis=0, tiled=True)  21.8 us
    all_to_all x1, blocking collectives, on_device(): lax.all_to_all(send_rows, 'sp', split_axis=0, concat_axis=0, tiled=True)  21.6 us
    all_gather x1, waiting for transfers between devices, on_device(): lax.all_gather(part_routed, 'tp', axis=1, tiled=True)  19.1 us
    all_to_all x1, blocking collectives, on_device(): lax.all_to_all(send_routed, 'sp', split_axis=0, concat_axis=0, tiled=True)  17.5 us
    all_gather x1, blocking collectives, on_device(): mix_grad = lax.all_gather(grad_stream, 'tp', axis=1, tiled=True)  8.42 us
    psum x1, blocking collectives, on_device(): lax.psum((jnp.sum(normed_grad, axis=1), jnp.sum(normed_grad * normed, axi...  6.95 us
  transfers between devices with their start and end apart: 7, of which 5 were waited for; matrix products, arithmetic and copies ran while one was open for 11% of the time, Pallas kernels for 0%

commit v1 on v0

--- a/solution.py
+++ b/solution.py
@@ -1,7 +1,16 @@
+import functools
 import jax
 import jax.numpy as jnp
 from jax import lax
 from jax.sharding import PartitionSpec as P
+
+
+def raise_pieces_all(block_here, which_axis, along_dim):
+    before = jnp.concatenate(jax.lax.all_gather(block_here, which_axis), axis=along_dim)
+    return before
+
+
+save_edge = functools.partial(raise_pieces_all, which_axis="tp", along_dim=1)
 
 
 def passed_along(value, axis, steps):
@@ -84,7 +93,7 @@
     )
     expert_rows, routed_rows = (
         lax.all_gather(part_rows, "tp", axis=1, tiled=True),
-        lax.all_gather(part_routed, "tp", axis=1, tiled=True),
+        save_edge(part_routed),
     )
     grad_up, grad_down, partial_rows = expert_backward(
         expert_rows, routed_rows, w_gate[0], w_up[0], w_down[0]

time: 253 us -> 255 us (level)
  waiting for transfers between devices: 115 us -> 119 us
  matrix products: 34.5 us -> 31.7 us
    all_gather x1, waiting for transfers between devices: 2.32 us -> 22.2 us  [on_device(): lax.all_gather(part_rows, 'tp', axis=1, tiled=True)]
    all_gather x1, waiting for transfers between devices: 19.1 us -> 2.32 us  [raise_pieces_all(): jax.lax.all_gather(block_here, which_axis)]
    all_to_all x1, blocking collectives: 21.6 us -> 17.5 us  [on_device(): lax.all_to_all(send_rows, 'sp', split_axis=0, concat_axis=0, tiled=True)]
    all_to_all x1, blocking collectives: 17.5 us -> 21.6 us  [on_device(): lax.all_to_all(send_routed, 'sp', split_axis=0, concat_axis=0, tiled=True)]
    dot_general x1, matrix products: 5.1 us -> 2.28 us  [expert_backward(): lax.dot_general(routed_rows, down_weight, (((1,), (1,)), ((), ())), prefe...]
  transfers between devices with their start and end apart: 7 -> 7, of which waited for: 5 -> 5; matrix products, arithmetic and copies ran while one was open for 11% -> 10% of each run, Pallas kernels for 0% -> 0%
where the time goes in v1:
time: 255 us
  waiting for transfers between devices  119 us (47%)
  blocking collectives  54.5 us (21%)
  matrix products  31.7 us (12%)
  local copies, waits for them, and re-layouts  19.4 us (8%)
  between operations  15.7 us (6%)
  other arithmetic  7.47 us (3%)
  starting transfers between devices  7.19 us (3%)
    reduce_scatter x1, waiting for transfers between devices, on_device(): lax.psum_scatter(lax.dot_general(columns, activated, (((0,), (0,)), ((),...  41.7 us
    reduce_scatter x1, waiting for transfers between devices, on_device(): lax.psum_scatter(partial_rows.astype(jnp.bfloat16).astype(jnp.float32).as...  30 us
    all_gather x1, waiting for transfers between devices, on_device(): lax.all_gather(part_rows, 'tp', axis=1, tiled=True)  22.2 us
    all_to_all x1, waiting for transfers between devices, on_device(): lax.all_to_all(shared, 'sp', split_axis=0, concat_axis=0, tiled=True)  21.8 us
    all_to_all x1, blocking collectives, on_device(): lax.all_to_all(send_routed, 'sp', split_axis=0, concat_axis=0, tiled=True)  21.6 us
    all_to_all x1, blocking collectives, on_device(): lax.all_to_all(send_rows, 'sp', split_axis=0, concat_axis=0, tiled=True)  17.5 us
    all_gather x1, blocking collectives, on_device(): mix_grad = lax.all_gather(grad_stream, 'tp', axis=1, tiled=True)  8.42 us
    psum x1, blocking collectives, on_device(): lax.psum((jnp.sum(normed_grad, axis=1), jnp.sum(normed_grad * normed, axi...  6.96 us
  transfers between devices with their start and end apart: 7, of which 5 were waited for; matrix products, arithmetic and copies ran while one was open for 10% of the time, Pallas kernels for 0%

profile of v1, /device:TPU:0, one launch (start us, length us, event | category | flops | bytes accessed | tf_op | source)
XLA Modules:
  0.0 254.5 jit_solution(7365819691560449141)
XLA Ops:
  8.1 0.8 copy.35
  8.9 0.1 eq.39
  9.0 0.1 reshape.207
  9.2 0.9 reduce-window.6
  10.0 0.2 slice_reduce_fusion
  10.3 0.1 fusion.113
  10.4 0.2 select_reduce_fusion
  10.6 0.2 fusion.15
  10.7 0.1 reduce_sum.55
  10.8 1.1 mul.435
  12.0 0.5 mul.436
  12.5 0.1 copy.37
  12.7 0.1 mul.433
  12.8 0.1 multiply_convert_fusion.5
  12.9 2.1 gather_fusion
  15.1 0.1 gather.19
  15.2 2.1 gather_fusion.1
  17.3 0.1 gather.21
  17.4 0.1 broadcast_in_dim.79
  17.5 0.3 select_select_fusion
  17.8 21.6 %all_to_all.27 = bf16[8,60,512]{2,1,0:T(8,128)(2,1)S(1)} all-to-all(bf16[8,60,512]{2,1,0:T(8,128)(2,1)S(1)} %get-tuple-element.45), channel_id=1, replica_groups=mesh['sp'=8,'tp'=4] {'sp'}, dimensions={0} | all-to-all | bytes 983040 | tf_op jit(solution)/shard_map/all_to_all | solution.py:92
  39.4 0.9 all_gather.15
  40.3 0.0 all-gather.6.cloned.1.call-start
  40.4 17.5 %all_to_all.28 = bf16[8,60,512]{2,1,0:T(8,128)(2,1)S(1)} all-to-all(bf16[8,60,512]{2,1,0:T(8,128)(2,1)S(1)} %get-tuple-element.44), channel_id=1, replica_groups=mesh['sp'=8,'tp'=4] {'sp'}, dimensions={0} | all-to-all | bytes 983040 | tf_op jit(solution)/shard_map/all_to_all | solution.py:91
  57.9 0.9 all_to_all.20
  58.8 0.2 reduce-scatter.3.cloned.1.call-start
  59.0 2.3 all-gather.4.cloned.1.call-done
  61.4 1.8 copy.42
  63.2 22.2 %all-gather.6.cloned.1.call-done = bf16[480,2048]{1,0:T(8,128)(2,1)} async-done(((bf16[480,512]{1,0:T(8,128)(2,1)}), bf16[480,2048]{1,0:T(8,128)(2,1)}) %all-gather.6.cloned.1.call-update) | async-done | bytes 1966096 | tf_op jit(solution)/shard_map/all_gather | solution.py:95
  85.4 5.0 %fusion.6 = f32[480,896]{1,0:T(8,128)S(1)} fusion(bf16[480,2048]{1,0:T(8,128)(2,1)} %all-gather.6.cloned.1.call-done, bf16[1,896,2048]{2,1,0:T(8,128)(2,1)} %param.18), kind=kOutput, calls=%fused_computation.39 | convolution fusion | flops 1761607680 | bytes 7356416 | tf_op jit(solution)/shard_map/dot_general | solution.py:27
  90.4 2.3 multiply_convert_fusion.2
  92.7 1.0 copy-done.18
  93.7 2.2 fusion
  95.9 2.3 fusion.2
  98.2 1.2 copy-done.17
  99.4 3.7 %add_convert_fusion = bf16[480,2048]{1,0:T(8,128)(2,1)} fusion(f32[480,2048]{1,0:T(8,128)S(1)} %fusion, bf16[1,896,2048]{2,1,0:T(8,128)(2,1)S(1)} %copy-done.12, f32[480,896]{1,0:T(8,128)S(1)} %fusion.6, f32[480,896]{1,0:T(8,128)S(1)} %get-tuple-element.47, f32[480,896]{1,0:T(8,128)S(1)} %fusion.2), kind=kOutput, calls=%fused_computation.32 | convolution fusion | flops 1767874560 | bytes 14729216 | tf_op jit(solution)/shard_map/dot_general | solution.py:47
  103.2 0.0 all-gather.8.cloned.1.call-start
  103.2 0.5 all-gather.8.cloned.1.call-update
  103.7 30.0 %reduce-scatter.3.cloned.1.call-done = bf16[480,512]{1,0:T(8,128)(2,1)} async-done(((bf16[480,2048]{1,0:T(8,128)(2,1)}), bf16[480,512]{1,0:T(8,128)(2,1)}) %reduce-scatter.3.cloned.1.call-update) | async-done | bytes 491536 | tf_op jit(solution)/shard_map/reduce_scatter | solution.py:101
  133.7 1.9 all_to_all.21
  135.6 5.5 %all-to-all-start.2 = ((bf16[8,60,512]{2,1,0:T(8,128)(2,1)}), bf16[8,60,512]{2,1,0:T(8,128)(2,1)S(1)}, u32[]{:S(2)}, u32[]{:S(2)}) async-start(bf16[8,60,512]{2,1,0:T(8,128)(2,1)} %all_to_all.21), calls=%async_computation.3 | async-start | bytes 1048576 | tf_op jit(solution)/shard_map/all_to_all | solution.py:107
  141.1 0.0 reduce-scatter.5.cloned.1.call-start
  141.2 0.1 reduce_sum.57
  141.3 0.1 copy.41
  141.5 0.1 mul.447
  141.6 0.1 copy.39
  141.7 0.2 copy.40
  141.9 21.8 %all-to-all-done.2 = bf16[8,60,512]{2,1,0:T(8,128)(2,1)S(1)} async-done(((bf16[8,60,512]{2,1,0:T(8,128)(2,1)}), bf16[8,60,512]{2,1,0:T(8,128)(2,1)S(1)}, u32[]{:S(2)}, u32[]{:S(2)}) %all-to-all-start.2) | async-done | bytes 491552 | tf_op jit(solution)/shard_map/all_to_all | solution.py:107
  163.7 0.1 all_to_all.23
  163.8 2.1 gather_fusion.2
  165.9 0.2 gather.23
  166.1 1.1 convert_reduce_fusion
  167.3 8.4 %all_gather.18 = bf16[192,2048]{1,0:T(8,128)(2,1)S(1)} all-gather(bf16[192,512]{1,0:T(8,128)(2,1)S(1)} %add_convert_fusion.1), channel_id=1, replica_groups=mesh['sp'=8,'tp'=4] {'tp'}, dimensions={1}, use_global_device_ids=true | all-gather | bytes 983040 | tf_op jit(solution)/shard_map/all_gather | solution.py:113
  175.7 2.3 convolution_convert_fusion
  178.0 0.8 copy-done.5
  178.9 6.0 %convert_bitcast_fusion = bf16[1,896,2048]{2,1,0:T(8,128)(2,1)} fusion(bf16[480,2048]{1,0:T(8,128)(2,1)S(1)} %bitcast.78, f32[480,896]{1,0:T(8,128)} %copy-done.17, f32[480,896]{1,0:T(8,128)} %copy-done.16), kind=kOutput, calls=%fused_computation.43 | convolution fusion | flops 1766023168 | bytes 9076736 | tf_op jit(solution)/shard_map/dot_general | solution.py:39
  184.9 2.5 fusion.121
  187.4 7.0 %all-reduce = (f32[192]{0:T(256)S(1)}, f32[192]{0:T(256)S(1)}) all-reduce(f32[192]{0:T(256)S(1)} %get-tuple-element.6, f32[192]{0:T(256)S(1)} %get-tuple-element.5), channel_id=1, replica_groups=mesh['sp'=8,'tp'=4] {'tp'}, use_global_device_ids=true, to_apply=%region_11.12 | all-reduce | flops 384 | bytes 3072 | tf_op jit(solution)/shard_map/psum | solution.py:134
  194.3 0.2 subtract_multiply_fusion
  194.5 1.3 collective-permute-start
  195.8 5.5 %convert_bitcast_fusion.1 = bf16[1,896,2048]{2,1,0:T(8,128)(2,1)} fusion(bf16[480,896]{1,0:T(8,128)(2,1)S(1)} %copy-done.19, bf16[480,2048]{1,0:T(8,128)(2,1)} %all-gather.6.cloned.1.call-done), kind=kOutput, calls=%fused_computation.44 | convolution fusion | flops 1763442688 | bytes 6496256 | tf_op jit(solution)/shard_map/dot_general | solution.py:44
  201.3 2.5 fusion.20
  203.8 41.7 %reduce-scatter.5.cloned.1.call-done = bf16[256,512]{1,0:T(8,128)(2,1)} async-done(((bf16[2048,512]{1,0:T(8,128)(2,1)}), bf16[256,512]{1,0:T(8,128)(2,1)}) %reduce-scatter.5.cloned.1.call-update) | async-done | bytes 262160 | tf_op jit(solution)/shard_map/reduce_scatter | solution.py:125
  245.6 1.8 convert_element_type.72
  (60 shorter events, 0.5 us)
Async XLA Ops:
  8.0 7.2 %copy-start = (bf16[192,512]{1,0:T(8,128)(2,1)S(1)}, bf16[192,512]{1,0:T(8,128)(2,1)}, u32[]{:S(2)}) copy-start(bf16[192,512]{1,0:T(8,128)(2,1)} %param.14) | copy-start | bytes 589828
  8.0 4.5 %copy-start.7 = (f32[192,2]{0,1:T(2,128)S(1)}, f32[192,2]{0,1:T(2,128)}, u32[]{:S(2)}) copy-start(f32[192,2]{0,1:T(2,128)} %param.17) | copy-start | bytes 4612
  8.0 53.3 %all-gather.4.cloned.1.call-start = ((), (), s32[]{:S(2)}) async-start(), calls=%async_computation.5 | async-start | bytes 2457600 | tf_op jit(solution)/shard_map/all_gather | solution.py:9
  40.3 45.0 %all-gather.6.cloned.1.call-start = ((), (), s32[]{:S(2)}) async-start(), calls=%async_computation.6 | async-start | bytes 2457600 | tf_op jit(solution)/shard_map/all_gather | solution.py:95
  58.8 74.9 %reduce-scatter.3.cloned.1.call-start = ((), (), s32[]{:S(2)}) async-start(), calls=%async_computation.7 | async-start | bytes 2457600 | tf_op jit(solution)/shard_map/reduce_scatter | solution.py:101
  85.3 5.0 %copy-start.10 = (bf16[1,896,2048]{2,1,0:T(8,128)(2,1)S(1)}, bf16[1,896,2048]{2,1,0:T(8,128)(2,1)}, u32[]{:S(2)}) copy-start(bf16[1,896,2048]{2,1,0:T(8,128)(2,1)} %param.20) | copy-start | bytes 11010052
  90.4 7.9 %copy-start.16 = (f32[480,896]{1,0:T(8,128)}, f32[480,896]{1,0:T(8,128)S(1)}, u32[]{:S(2)}) copy-start(f32[480,896]{1,0:T(8,128)S(1)} %fusion.6) | copy-start | bytes 5160964
  90.4 3.3 %copy-start.11 = (bf16[1,896,2048]{2,1,0:T(8,128)(2,1)S(1)}, bf16[1,896,2048]{2,1,0:T(8,128)(2,1)}, u32[]{:S(2)}) copy-start(bf16[1,896,2048]{2,1,0:T(8,128)(2,1)} %param.19) | copy-start | bytes 11010052
  92.7 1.0 copy-start.18
  93.7 2.2 copy-start.13
  95.9 3.5 %copy-start.12 = (bf16[1,896,2048]{2,1,0:T(8,128)(2,1)S(1)}, bf16[1,896,2048]{2,1,0:T(8,128)(2,1)}, u32[]{:S(2)}) copy-start(bf16[1,896,2048]{2,1,0:T(8,128)(2,1)} %param.18) | copy-start | bytes 11010052
  98.2 1.2 copy-start.17
  103.1 38.2 %copy-start.6 = (s32[192,2]{0,1:T(2,128)S(1)}, s32[192,2]{0,1:T(2,128)}, u32[]{:S(2)}) copy-start(s32[192,2]{0,1:T(2,128)} %param.16) | copy-start | bytes 4612
  103.2 81.8 %all-gather.8.cloned.1.call-start = ((), (), s32[]{:S(2)}) async-start(), calls=%async_computation.9 | async-start | bytes 2359296 | tf_op jit(solution)/shard_map/all_gather | solution.py:121
  135.6 28.1 %all-to-all-start.2 = ((bf16[8,60,512]{2,1,0:T(8,128)(2,1)}), bf16[8,60,512]{2,1,0:T(8,128)(2,1)S(1)}, u32[]{:S(2)}, u32[]{:S(2)}) async-start(bf16[8,60,512]{2,1,0:T(8,128)(2,1)} %all_to_all.21), calls=%async_computation.3 | async-start | bytes 1048576 | tf_op jit(solution)/shard_map/all_to_all | solution.py:107
  141.1 104.5 %reduce-scatter.5.cloned.1.call-start = ((), (), s32[]{:S(2)}) async-start(), calls=%async_computation.8 | async-start | bytes 2359296 | tf_op jit(solution)/shard_map/reduce_scatter | solution.py:125
  163.8 3.4 %copy-start.1 = (bf16[192,512]{1,0:T(8,128)(2,1)S(1)}, bf16[192,512]{1,0:T(8,128)(2,1)}, u32[]{:S(2)}) copy-start(bf16[192,512]{1,0:T(8,128)(2,1)} %param.15) | copy-start | bytes 589828
  165.9 9.8 %copy-start.8 = (f32[192]{0:T(256)S(1)}, f32[192]{0:T(256)}, u32[]{:S(2)}) copy-start(f32[192]{0:T(256)} %param.23) | copy-start | bytes 2308
  165.9 9.8 %copy-start.9 = (f32[192]{0:T(256)S(1)}, f32[192]{0:T(256)}, u32[]{:S(2)}) copy-start(f32[192]{0:T(256)} %param.22) | copy-start | bytes 2308
  165.9 9.8 %copy-start.14 = (f32[512]{0:T(512)S(1)}, f32[512]{0:T(512)}, u32[]{:S(2)}) copy-start(f32[512]{0:T(512)} %param.25) | copy-start | bytes 6148
  165.9 9.8 %copy-start.15 = (f32[512]{0:T(512)S(1)}, f32[512]{0:T(512)}, u32[]{:S(2)}) copy-start(f32[512]{0:T(512)} %param.24) | copy-start | bytes 6148
  166.1 9.7 %copy-start.3 = (bf16[192,512]{1,0:T(8,128)(2,1)S(1)}, bf16[192,512]{1,0:T(8,128)(2,1)}, u32[]{:S(2)}) copy-start(bf16[192,512]{1,0:T(8,128)(2,1)} %param.21) | copy-start | bytes 589828
  167.3 10.7 %copy-start.2 = (bf16[192,512]{1,0:T(8,128)(2,1)}, bf16[192,512]{1,0:T(8,128)(2,1)S(1)}, u32[]{:S(2)}) copy-start(bf16[192,512]{1,0:T(8,128)(2,1)S(1)} %add_convert_fusion.1) | copy-start | bytes 589828
  178.0 0.8 copy-start.5
  178.9 6.0 %copy-start.4 = (bf16[192,512]{1,0:T(8,128)(2,1)S(1)}, bf16[192,512]{1,0:T(8,128)(2,1)}, u32[]{:S(2)}) copy-start(bf16[192,512]{1,0:T(8,128)(2,1)} %param.21) | copy-start | bytes 589828
  184.9 10.9 %copy-start.19 = (bf16[480,896]{1,0:T(8,128)(2,1)S(1)}, bf16[480,896]{1,0:T(8,128)(2,1)}, u32[]{:S(2)}) copy-start(bf16[480,896]{1,0:T(8,128)(2,1)} %copy-done.18) | copy-start | bytes 2580484
  194.5 6.8 %collective-permute-start = (f32[30,512]{1,0:T(8,128)S(1)}, f32[30,512]{1,0:T(8,128)S(1)}, u32[]{:S(2)}, u32[]{:S(2)}) collective-permute-start(f32[30,512]{1,0:T(8,128)S(1)} %slice.263), channel_id=1, source_target_pairs={{4,0},{8,4},{12,8},{16,12},{20,16},{24,20},{28,24},{5,1},{9,5},{13... | collective-permute-start | bytes 184328 | tf_op jit(solution)/shard_map/ppermute | solution.py:19
Sparse Core Ops, SparseCore 0:
  40.4 20.8 all-gather.3
  63.5 21.8 all-gather.5
  103.3 30.3 reduce-scatter.2
Sparse Core Ops, SparseCore 1:
  105.8 58.3 all-gather.7
  178.1 67.4 reduce-scatter.4
